TPU v7x, 512 devices: a 4x2x32 block of a 4x8x32 slice. The times are simulated.
512 devices in a mesh: grp: 2 (over y), sp: 32 (over z), tp: 8 (over x, core).
Axes of the slice: x: 4, y: 2, z: 32, core: 2. Of those that a mesh axis runs over, the one named last changes fastest.
The devices are a block of a 4x8x32 slice.
Arguments:
- tokens: bfloat16 [24576, 2048], P(('grp', 'sp'), 'tp'), parts along dimension 0, may hold values from -6 to 6
- norm_gain: float32 [2048], replicated, may hold values from 0.1 to 1.9
- qk_gain: float32 [4, 64], replicated, may hold values from 0.7 to 5.5
- w_query_window: bfloat16 [2048, 1024], P('sp', 'tp'), may hold values from -1 to 1
- w_key_window: bfloat16 [2048, 512], P('sp', 'tp'), may hold values from -1 to 1
- w_value_window: bfloat16 [2048, 512], P('sp', 'tp'), may hold values from -0.125 to 0.125
- sink_logits: float32 [16], P('tp'), may hold values from 0 to 5
- w_query_forget: bfloat16 [2048, 1024], P('sp', 'tp'), may hold values from -1 to 1
- w_key_forget: bfloat16 [2048, 1024], P('sp', 'tp'), may hold values from -1 to 1
- w_value_forget: bfloat16 [2048, 1024], P('sp', 'tp'), may hold values from -0.125 to 0.125
- gate_cum: float32 [24576, 16], P(('grp', 'sp'), 'tp'), parts along dimension 0, as said below
- w_merge: bfloat16 [2048, 2, 2048], P('sp', None, 'tp'), may hold values from -0.125 to 0.125
- w_branch: bfloat16 [2, 1024, 2048], P(None, 'sp', 'tp'), may hold values from -0.8984375 to 0.8984375
Outputs:
- mixed: bfloat16 [24576, 2048], P(('grp', 'sp'), 'tp'), parts along dimension 0
There are 2 independent parts, one for each index of `grp`. A program takes and returns all parts, laid end to end along the dimension named above; an argument that names none is the same for every part. Nothing has to cross between parts.
Inputs may be any that keep to these rules, and one draw needn't show every extreme that they name: `gate_cum`: along positions each head's values never rise.
All inputs are finite; a program needn't handle non-finite values.
Results may differ from a plain program's by a relative error of at most 0.012.
Values may be sent and summed in bfloat16 or wider, within the bound.
A program may use at most 64 MiB of HBM per device.

v0:
```python
import math

import jax
import jax.numpy as jnp
from jax import lax
from jax.sharding import PartitionSpec as P

HEAD = 64
WINDOW = 128


epsilon = 1e-06
big_negative = -1e30


def sent_together(arrays, axis, dim, along):
    widths = [a.shape[along] for a in arrays]
    both = jnp.concatenate(arrays, axis=along)
    filled = lax.all_gather(both, axis, axis=dim, tiled=True)
    return tuple(jnp.split(filled, [sum(widths[:k]) for k in range(1, len(widths))], axis=along))


def in_order(tiles, dim):
    dims = list(tiles.shape[1:])
    dims[dim] *= tiles.shape[0]
    return jnp.moveaxis(tiles, 0, dim).reshape(dims)


def sent_to_all(value, axis):
    size = lax.axis_size(axis)
    return lax.all_to_all(
        jnp.broadcast_to(value[None], (size, *value.shape)), axis, 0, 0, tiled=True
    )


def gather_directly(value, axis, dim):
    return in_order(sent_to_all(value, axis), dim)


def from_behind(value, axis, by):
    size = lax.axis_size(axis)
    pairs = [(i, i + by) for i in range(size) if 0 <= i + by < size]
    return lax.ppermute(value, axis, pairs)


def head_norm(raw, gain, head_count):
    split = raw.reshape(raw.shape[0], head_count, -1)
    scaled = split * lax.rsqrt(jnp.mean(split * split, axis=-1, keepdims=True) + epsilon) * gain
    return scaled.astype(jnp.bfloat16)


def window_attend(queries, keys_ext, values_ext, sink_rows, first_pos):
    row_count, head_count, head_size = queries.shape
    group_count = keys_ext.shape[1]
    span_rows = WINDOW // 2
    block_count = row_count // span_rows
    query_blocks = queries.reshape(
        block_count, span_rows, group_count, head_count // group_count, head_size
    )
    key_blocks = jnp.concatenate(
        [
            keys_ext[lag_index * span_rows : lag_index * span_rows + row_count].reshape(
                block_count, span_rows, group_count, head_size
            )
            for lag_index in range(3)
        ],
        axis=1,
    )
    value_blocks = jnp.concatenate(
        [
            values_ext[lag_index * span_rows : lag_index * span_rows + row_count].reshape(
                block_count, span_rows, group_count, head_size
            )
            for lag_index in range(3)
        ],
        axis=1,
    )
    scores = jnp.einsum(
        "nqgrd,nkgd->ngrqk", query_blocks, key_blocks, preferred_element_type=jnp.float32
    ) * head_size ** (-0.5)
    distance = WINDOW + jnp.arange(span_rows)[:, None] - jnp.arange(3 * span_rows)[None, :]
    key_pos = (
        first_pos
        - WINDOW
        + jnp.arange(block_count)[:, None] * span_rows
        + jnp.arange(3 * span_rows)[None, :]
    )
    is_valid = ((distance >= 0) & (distance < WINDOW))[None] & (key_pos >= 0)[:, None, :]
    is_valid = is_valid[:, None, None]
    sink_grid = sink_rows.reshape(1, group_count, head_count // group_count, 1)
    row_max = jnp.maximum(jnp.max(jnp.where(is_valid, scores, big_negative), axis=-1), sink_grid)
    weights = jnp.where(is_valid, jnp.exp(scores - row_max[..., None]), 0.0)
    row_total = jnp.sum(weights, axis=-1) + jnp.exp(sink_grid - row_max)
    prob_rows = (weights / row_total[..., None]).astype(jnp.bfloat16)
    mixed_sum = jnp.einsum(
        "ngrqk,nkgd->nqgrd", prob_rows, value_blocks, preferred_element_type=jnp.float32
    )
    return mixed_sum.reshape(row_count, head_count * head_size).astype(jnp.bfloat16)


def forget_groups(groups, keys, values, gates):
    head_count, head_size = (keys.shape[1], keys.shape[2])
    gates_all = lax.all_gather(gates, "sp", axis=0, tiled=True)

    def absorber(queries, query_gate, query_pos):

        def absorb(running, block):
            row_max, row_total, mixed_sum = running
            key_rows, value_rows, key_gate, key_pos = block
            scores = jnp.einsum(
                "qhd,khd->hqk", queries, key_rows, preferred_element_type=jnp.float32
            ) * head_size ** (-0.5)
            scores = scores + query_gate.T[:, :, None] - key_gate.T[:, None, :]
            is_valid = (query_pos[:, None] >= key_pos[None, :])[None]
            new_max = jnp.maximum(
                row_max, jnp.max(jnp.where(is_valid, scores, big_negative), axis=-1)
            )
            weights = jnp.where(is_valid, jnp.exp(scores - new_max[..., None]), 0.0)
            shrink = jnp.exp(row_max - new_max)
            row_total = row_total * shrink + jnp.sum(weights, axis=-1)
            mixed_sum = mixed_sum * shrink.T[:, :, None] + jnp.einsum(
                "hqk,khd->qhd",
                weights.astype(jnp.bfloat16),
                value_rows,
                preferred_element_type=jnp.float32,
            )
            return ((new_max, row_total, mixed_sum), None)

        return absorb

    initial = tuple(
        (
            (
                jnp.full((head_count, group[0].shape[0]), big_negative, jnp.float32),
                jnp.zeros((head_count, group[0].shape[0]), jnp.float32),
                jnp.zeros((group[0].shape[0], head_count, head_size), jnp.float32),
            )
            for group in groups
        )
    )
    first_row = jnp.int32(0)
    key_rows, value_rows = sent_together((keys, values), "sp", 0, 1)
    piece_rows = key_rows.shape[0]
    sub_rows = math.gcd(piece_rows, 2048)
    turns = piece_rows // sub_rows
    key_gate = gates_all
    key_pos = jnp.arange(piece_rows)
    blocks = (
        key_rows.reshape(turns, sub_rows, head_count, head_size),
        value_rows.reshape(turns, sub_rows, head_count, head_size),
        key_gate.reshape(turns, sub_rows, head_count),
        key_pos.reshape(turns, sub_rows),
    )
    updated = []
    for (queries, query_gate, query_pos), state in zip(groups, initial):
        absorb = absorber(queries, query_gate, query_pos)

        def advance(current):
            return lax.scan(absorb, current, blocks)[0]

        def keep(current):
            return current

        updated.append(lax.cond(first_row <= query_pos[-1], advance, keep, state))
    finals = tuple(updated)
    return [
        (mixed_sum / row_total.T[:, :, None])
        .reshape(mixed_sum.shape[0], head_count * head_size)
        .astype(jnp.bfloat16)
        for row_max, row_total, mixed_sum in finals
    ]


def on_device(
    tokens,
    norm_gain,
    qk_gain,
    w_query_window,
    w_key_window,
    w_value_window,
    sink_logits,
    w_query_forget,
    w_key_forget,
    w_value_forget,
    gate_cum,
    w_merge,
    w_branch,
):
    row_count = tokens.shape[0]
    row_offset = lax.axis_index("sp") * row_count
    gathered = gather_directly(tokens, "tp", 1)
    as_float = gathered.astype(jnp.float32)
    normed = (
        as_float
        * lax.rsqrt(jnp.mean(as_float * as_float, axis=-1, keepdims=True) + epsilon)
        * norm_gain
    ).astype(jnp.bfloat16)
    merge_flat = w_merge.reshape(w_merge.shape[0], -1)
    pieces = sent_together(
        (
            w_query_window,
            w_key_window,
            w_value_window,
            w_query_forget,
            w_key_forget,
            w_value_forget,
            merge_flat,
        ),
        "sp",
        0,
        1,
    )
    projected = tuple(
        (jnp.dot(normed, weight_rows, preferred_element_type=jnp.float32) for weight_rows in pieces)
    )
    query_heads = w_query_window.shape[1] // HEAD
    group_heads = w_key_window.shape[1] // HEAD
    window_query = head_norm(projected[0], qk_gain[0], query_heads)
    window_key = head_norm(projected[1], qk_gain[1], group_heads)
    window_value = projected[2].astype(jnp.bfloat16).reshape(row_count, group_heads, HEAD)
    prev_key, prev_value = from_behind(
        (window_key[row_count - WINDOW :], window_value[row_count - WINDOW :]), "sp", 1
    )
    window_out = window_attend(
        window_query,
        jnp.concatenate([prev_key, window_key], axis=0),
        jnp.concatenate([prev_value, window_value], axis=0),
        sink_logits,
        row_offset,
    )
    forget_query = head_norm(projected[3], qk_gain[2], query_heads)
    forget_key = head_norm(projected[4], qk_gain[3], query_heads)
    forget_value = projected[5].astype(jnp.bfloat16).reshape(row_count, query_heads, HEAD)
    own_pos = row_offset + jnp.arange(row_count)
    forget_out = forget_groups(
        [(forget_query, gate_cum, own_pos)], forget_key, forget_value, gate_cum
    )[0]
    channel_count = w_merge.shape[2]
    merge_gate = jax.nn.sigmoid(projected[6]).reshape(row_count, 2, channel_count)
    branch_full = lax.all_gather(w_branch, "sp", axis=1, tiled=True)
    head_stack = jnp.stack([window_out, forget_out], axis=1)
    weight_rows = branch_full
    projection = jnp.einsum(
        "uxa,xag->uxg",
        gather_directly(head_stack, "tp", 2),
        weight_rows,
        preferred_element_type=jnp.float32,
    )
    return (merge_gate[:, 0] * projection[:, 0] + merge_gate[:, 1] * projection[:, 1]).astype(
        jnp.bfloat16
    )


def solution(mesh):
    return jax.shard_map(
        on_device,
        mesh=mesh,
        in_specs=(
            P(("grp", "sp"), "tp"),
            P(),
            P(),
            P("sp", "tp"),
            P("sp", "tp"),
            P("sp", "tp"),
            P("tp"),
            P("sp", "tp"),
            P("sp", "tp"),
            P("sp", "tp"),
            P(("grp", "sp"), "tp"),
            P("sp", None, "tp"),
            P(None, "sp", "tp"),
        ),
        out_specs=P(("grp", "sp"), "tp"),
        check_vma=False,
    )
```

profile of v0, /device:TPU:34, one launch (start us, length us, event | category | flops | bytes accessed | tf_op | source)
XLA Modules:
  0.0 458.4 jit_solution(7849762737389114048)
XLA Ops:
  6.6 0.9 copy.129
  7.4 1.6 concatenate.18
  9.0 2.2 broadcast_in_dim.89
  11.2 43.9 %all-to-all-start = ((bf16[8,384,256]{2,1,0:T(8,128)(2,1)}), bf16[8,384,256]{2,1,0:T(8,128)(2,1)S(1)}, u32[]{:S(2)}, u32[]{:S(2)}) async-start(bf16[8,384,256]{2,1,0:T(8,128)(2,1)} %broadcast_in_dim.89), calls=%async_computation | async-start | bytes 3145728 | tf_op jit(solution)/shard_map/all_to_all | solution.py:31
  55.7 19.6 %all-to-all-done = bf16[8,384,256]{2,1,0:T(8,128)(2,1)S(1)} async-done(((bf16[8,384,256]{2,1,0:T(8,128)(2,1)}), bf16[8,384,256]{2,1,0:T(8,128)(2,1)S(1)}, u32[]{:S(2)}, u32[]{:S(2)}) %all-to-all-start) | async-done | bytes 1572896 | tf_op jit(solution)/shard_map/all_to_all | solution.py:31
  75.3 0.9 copy.96
  77.1 1.6 fusion.27
  78.6 97.4 %all-gather.4.cloned.1.call-done = bf16[2048,1152]{1,0:T(8,128)(2,1)} async-done(((bf16[64,1152]{1,0:T(8,128)(2,1)}), bf16[2048,1152]{1,0:T(8,128)(2,1)}) %all-gather.4.cloned.1.call-update) | async-done | bytes 4718608 | tf_op jit(solution)/shard_map/all_gather | solution.py:19
  176.0 2.3 slice_bitcast_fusion.2
  178.3 1.2 copy.108
  180.1 2.0 convolution_convert_fusion.1
  182.1 0.7 pad_maximum_fusion
  182.9 0.7 all-gather.8.cloned.1.call-update
  185.2 57.9 %all_gather.14 = f32[12288,2]{0,1:T(2,128)} all-gather(f32[384,2]{0,1:T(2,128)S(1)} %copy-done.3), channel_id=1, replica_groups=mesh['grp'=2,'sp'=32,'tp'=8] {'sp'}, dimensions={0}, use_global_device_ids=true | all-gather | bytes 101376 | tf_op jit(solution)/shard_map/all_gather | solution.py:103
  243.2 2.2 convolution_convert_fusion.2
  246.0 3.2 collective-permute-start
  249.3 1.9 multiply_reduce_fusion.4
  252.0 2.0 collective-permute-start.1
  254.7 0.7 multiply_convert_fusion.3
  255.4 1.3 multiply_convert_fusion.1
  257.3 0.9 fusion.72
  259.5 0.9 fusion.73
  261.5 60.5 %all-gather.6.cloned.1.call-done = bf16[12288,4,64]{0,2,1:T(8,128)(2,1)} async-done(((bf16[384,4,64]{0,2,1:T(8,128)(2,1)}), bf16[12288,4,64]{0,2,1:T(8,128)(2,1)}) %all-gather.6.cloned.1.call-update) | async-done | bytes 6291472 | tf_op jit(solution)/shard_map/all_gather | solution.py:19
  322.0 72.8 %conditional.1 = (f32[2,384]{1,0:T(2,128)}, f32[384,2,64]{0,2,1:T(8,128)}) conditional(s32[]{:T(128)} %bitcast.26, () %tuple.20, (bf16[12288,4,64]{0,2,1:T(8,128)(2,1)}, f32[12288,2]{0,1:T(2,128)}, s32[6,2048]{1,0:T(8,128)S(1)}, s32[6,2048]{1,0:T(8,128)S(1)}, s32[384]{0:T(512)S(1)}, /*index=5*/bf16[384,2,64]{0,2,1:T(8,128)(2,1)}, ...), branch_computations={%region_7.8_spmd, %region_8.13_spmd} | conditional | flops 430354944 | bytes 49433404 | solution.py:164
  322.3 3.3 fusion.78
  325.5 2.6 copy_bitcast_fusion
  328.1 66.7 %while.18 = (s32[]{:T(128)}, f32[2,384]{1,0:T(2,128)S(1)}, f32[2,384]{1,0:T(2,128)}, f32[384,2,64]{0,2,1:T(8,128)}, s32[384]{0:T(512)S(1)}, /*index=5*/s32[6,204...) while((s32[]{:T(128)}, f32[2,384]{1,0:T(2,128)S(1)}, ...), condition=%wide.region_12.12_spmd.clone, body=%wide.region_9.11_spmd.clone.sunk | while | flops 430330368 | bytes 23726752 | solution.py:159
  328.1 0.7 dynamic-slice_bitcast_fusion.2
  329.5 3.1 fusion.105
  332.6 2.0 fusion.107
  334.5 2.8 fusion.109
  337.9 0.7 dynamic-slice_bitcast_fusion.2
  339.2 3.1 fusion.105
  342.3 2.0 fusion.107
  344.3 3.7 fusion.109
  348.0 1.3 fusion.108
  349.3 0.7 dynamic-slice_bitcast_fusion.2
  350.6 3.1 fusion.105
  353.7 2.0 fusion.107
  355.7 3.7 fusion.109
  359.4 1.3 fusion.108
  360.7 0.7 dynamic-slice_bitcast_fusion.2
  362.0 3.1 fusion.105
  365.1 2.0 fusion.107
  367.0 3.7 fusion.109
  370.7 1.3 fusion.108
  372.1 0.7 dynamic-slice_bitcast_fusion.2
  373.4 3.1 fusion.105
  376.5 2.0 fusion.107
  378.4 3.7 fusion.109
  382.1 1.3 fusion.108
  383.4 0.7 dynamic-slice_bitcast_fusion.2
  384.7 3.1 fusion.105
  387.8 2.0 fusion.107
  389.8 3.7 fusion.109
  393.5 1.3 fusion.108
  394.8 1.1 divide_convert_fusion.2
  396.0 1.5 broadcast_in_dim.93
  397.5 4.6 all-to-all-start.1
  402.1 3.7 fusion.47
  405.7 1.6 reshape.322
  408.0 41.3 %all-gather.8.cloned.1.call-done = bf16[2,1024,256]{2,1,0:T(8,128)(2,1)} async-done(((bf16[2,32,256]{2,1,0:T(8,128)(2,1)}), bf16[2,1024,256]{2,1,0:T(8,128)(2,1)}) %all-gather.8.cloned.1.call-update) | async-done | bytes 1048592 | tf_op jit(solution)/shard_map/all_gather | solution.py:240
  449.3 1.8 fusion.39
  451.1 0.8 fusion.59
  (104 shorter events, 12.9 us)
Async XLA Ops:
  6.5 48.6 %copy-start.5 = (f32[2048]{0:T(1024)S(1)}, f32[2048]{0:T(1024)}, u32[]{:S(2)}) copy-start(f32[2048]{0:T(1024)} %param.18) | copy-start | bytes 24580
  6.5 48.6 %copy-start.7 = (f32[4,64]{1,0:T(4,128)S(1)}, f32[4,64]{1,0:T(4,128)}, u32[]{:S(2)}) copy-start(f32[4,64]{1,0:T(4,128)} %param.19) | copy-start | bytes 3076
  6.6 169.4 %all-gather.4.cloned.1.call-start = ((), (), s32[]{:S(2)}) async-start(), calls=%async_computation.2 | async-start | bytes 4866048 | tf_op jit(solution)/shard_map/all_gather | solution.py:19
  11.2 64.1 %all-to-all-start = ((bf16[8,384,256]{2,1,0:T(8,128)(2,1)}), bf16[8,384,256]{2,1,0:T(8,128)(2,1)S(1)}, u32[]{:S(2)}, u32[]{:S(2)}) async-start(bf16[8,384,256]{2,1,0:T(8,128)(2,1)} %broadcast_in_dim.89), calls=%async_computation | async-start | bytes 3145728 | tf_op jit(solution)/shard_map/all_to_all | solution.py:31
  55.2 266.8 %all-gather.6.cloned.1.call-start = ((), (), s32[]{:S(2)}) async-start(), calls=%async_computation.3 | async-start | bytes 6488064 | tf_op jit(solution)/shard_map/all_gather | solution.py:19
  179.5 5.7 %copy-start.3 = (f32[384,2]{0,1:T(2,128)S(1)}, f32[384,2]{0,1:T(2,128)}, u32[]{:S(2)}) copy-start(f32[384,2]{0,1:T(2,128)} %param.27) | copy-start | bytes 9220
  182.9 266.4 %all-gather.8.cloned.1.call-start = ((), (), s32[]{:S(2)}) async-start(), calls=%async_computation.4 | async-start | bytes 1081344 | tf_op jit(solution)/shard_map/all_gather | solution.py:240
  245.4 5.8 %copy-start.1 = (bf16[384,64]{0,1:T(8,128)(2,1)}, bf16[384,64]{0,1:T(8,128)(2,1)S(1)}, u32[]{:S(2)}) copy-start(bf16[384,64]{0,1:T(8,128)(2,1)S(1)} %convolution_convert_fusion.2) | copy-start | bytes 147460
  246.0 13.5 %collective-permute-start = (bf16[128,1,64]{0,2,1:T(8,128)(2,1)}, bf16[128,1,64]{0,2,1:T(8,128)(2,1)}, u32[]{:S(2)}, u32[]{:S(2)}) collective-permute-start(bf16[128,1,64]{0,2,1:T(8,128)(2,1)} %slice_bitcast_fusion.4), channel_id=1, source_target_pairs={{0,8},{8,16},{16,24},{24,32},{32,40},{40,48},{48,56},{56,64},{64,7... | collective-permute-start | bytes 49160 | tf_op jit(solution)/shard_map/ppermute | solution.py:43
  251.9 5.1 %copy-start.2 = (bf16[384,64]{0,1:T(8,128)(2,1)S(1)}, bf16[384,64]{0,1:T(8,128)(2,1)}, u32[]{:S(2)}) copy-start(bf16[384,64]{0,1:T(8,128)(2,1)} %copy-done.1) | copy-start | bytes 147460
  252.0 5.3 %collective-permute-start.1 = (bf16[128,1,64]{0,2,1:T(8,128)(2,1)S(1)}, bf16[128,1,64]{0,2,1:T(8,128)(2,1)}, u32[]{:S(2)}, u32[]{:S(2)}) collective-permute-start(bf16[128,1,64]{0,2,1:T(8,128)(2,1)S(1)} %slice_bitcast_fusion.3), channel_id=1, source_target_pairs={{0,8},{8,16},{16,24},{24,32},{32,40},{40,48},{48,56},{56,64},{64,7... | collective-permute-start | bytes 49160 | tf_op jit(solution)/shard_map/ppermute | solution.py:43
  254.2 4.8 %copy-start.6 = (f32[2]{0:T(128)S(1)}, f32[2]{0:T(128)}, u32[]{:S(2)}) copy-start(f32[2]{0:T(128)} %param.23) | copy-start | bytes 28
  325.5 2.6 copy-start.4
  394.8 7.3 %copy-start = (bf16[384,2048]{0,1:T(8,128)(2,1)S(1)}, bf16[384,2048]{0,1:T(8,128)(2,1)}, u32[]{:S(2)}) copy-start(bf16[384,2048]{0,1:T(8,128)(2,1)} %fusion.27) | copy-start | bytes 4718596
  397.5 51.8 %all-to-all-start.1 = ((bf16[8,384,2,128]{3,1,2,0:T(8,128)(2,1)}), bf16[8,384,2,128]{3,1,2,0:T(8,128)(2,1)S(1)}, u32[]{:S(2)}, u32[]{:S(2)}) async-start(bf16[8,384,2,128]{3,1,2,0:T(8,128)(2,1)} %broadcast_in_dim.93), calls=%async_computation.1 | async-start | bytes 3145728 | tf_op jit(solution)/shard_map/all_to_all | solution.py:31
Sparse Core Ops, SparseCore 0:
  9.4 166.5 all-gather.3
  183.0 138.9 all-gather.5
  324.1 125.1 all-gather.7
where the time goes:
time: 460 us; the launch traced here: 458 us
  waiting for transfers between devices  220 us (48%)
  blocking collectives  57.9 us (13%)
  starting transfers between devices  53.8 us (12%)
  matrix products  53.5 us (12%)
  other arithmetic  32.1 us (7%)
  local copies, waits for them, and re-layouts  26.7 us (6%)
  between operations  14.3 us (3%)
    all_gather x2, waiting for transfers between devices, sent_together(): filled = lax.all_gather(both, axis, axis=dim, tiled=True)  158 us
    all_gather x1, blocking collectives, forget_groups(): gates_all = lax.all_gather(gates, 'sp', axis=0, tiled=True)  57.9 us
    all_to_all x2, starting transfers between devices, sent_to_all(): lax.all_to_all(jnp.broadcast_to(value[None], (size, *value.shape)), axis,...  48.5 us
    all_gather x1, waiting for transfers between devices, on_device(): branch_full = lax.all_gather(w_branch, 'sp', axis=1, tiled=True)  41.3 us
    dot_general x6, matrix products, absorb(): jnp.einsum('hqk,khd->qhd', weights.astype(jnp.bfloat16), value_rows, pref...  21.3 us
    all_to_all x2, waiting for transfers between devices, sent_to_all(): lax.all_to_all(jnp.broadcast_to(value[None], (size, *value.shape)), axis,...  19.6 us
    dot_general x6, matrix products, absorb(): jnp.einsum('qhd,khd->hqk', queries, key_rows, preferred_element_type=jnp....  18.4 us
    reduce_sum x6, other arithmetic, absorb(): row_total = row_total * shrink + jnp.sum(weights, axis=-1)  11.8 us
  transfers between devices with their start and end apart: 7, of which 4 were waited for; matrix products, arithmetic and copies ran while one was open for 22% of the time, Pallas kernels for 0%

commit v1 on v0

v1 whole, which is shorter than its diff:
```python
import functools
import math

import jax
import jax.numpy as jnp
from jax import lax
from jax.experimental import pallas as pl
from jax.experimental.pallas import tpu as pltpu
from jax.sharding import PartitionSpec as P

HEAD = 64
PAIR = 2 * HEAD
WINDOW = 128
MESH = pl.DeviceIdType.MESH

epsilon = 1e-06
big_negative = -1e30
log2e = math.log2(math.e)


def low_half(shape):
    return lax.broadcasted_iota(jnp.int32, shape, 1) < HEAD


def pair_norm(raw, gain):
    low = low_half(raw.shape)
    squares = raw * raw
    first = jnp.sum(jnp.where(low, squares, 0.0), axis=1, keepdims=True)
    second = jnp.sum(jnp.where(low, 0.0, squares), axis=1, keepdims=True)
    mean = jnp.where(low, first, second) * (1.0 / HEAD)
    return raw * lax.rsqrt(mean + epsilon) * gain


def dot_nt(a, b):
    return lax.dot_general(a, b, (((1,), (1,)), ((), ())), preferred_element_type=jnp.float32)


class TpGather:
    def __init__(self, source, buf, t, chips, sems):
        self.source, self.buf, self.chips = source, buf, chips
        self.send, self.recv, self.relay_send, self.relay_recv = sems
        self.t, self.x, self.core = t, t // 2, t % 2
        self.steps = chips // 2
        self.half = buf.shape[1] // 2

    def slot(self, x, core):
        return lax.rem(x + 2 * self.chips, self.chips) * 2 + core

    def block(self, d, s):
        return self.slot(self.x - s if d == 0 else self.x + s, self.core)

    def parts(self, d, s):
        return (0, 1) if s < self.steps - 1 else (d,)

    def ring(self, d, s, c):
        block = self.block(d, s)
        rows = pl.ds(c * self.half, self.half)
        dst = self.buf.at[block, rows]
        src = self.source.at[rows] if s == 0 and self.source is not None else dst
        peer = self.slot(self.x + (1 if d == 0 else -1), self.core)
        return pltpu.make_async_remote_copy(
            src_ref=src,
            dst_ref=dst,
            send_sem=self.send.at[d, s, c],
            recv_sem=self.recv.at[d, s, c],
            device_id={"tp": peer},
            device_id_type=MESH,
        )

    def relay(self, k, block):
        dst = self.buf.at[block]
        src = self.source if k == 0 and self.source is not None else dst
        return pltpu.make_async_remote_copy(
            src_ref=src,
            dst_ref=dst,
            send_sem=self.relay_send.at[k],
            recv_sem=self.relay_recv.at[k],
            device_id={"tp": self.t + 1 - 2 * self.core},
            device_id_type=MESH,
        )

    def relays(self):
        order = [(0, 0)]
        for s in range(self.steps - 1):
            order += [(1 + 2 * s, -(s + 1)), (2 + 2 * s, s + 1)]
        return order + [(self.chips - 1, self.steps)]

    def begin(self):
        for d in (0, 1):
            for c in self.parts(d, 0):
                self.ring(d, 0, c).start()
        self.relay(0, self.slot(self.x, self.core)).start()

    def advance(self, s):
        for d in (0, 1):
            for c in self.parts(d, s):
                self.ring(d, s, c).wait_recv()
                if s + 1 < self.steps and c in self.parts(d, s + 1):
                    self.ring(d, s + 1, c).start()
        if s + 1 < self.steps:
            self.relay(1 + 2 * s, self.slot(self.x - s - 1, self.core)).start()
            self.relay(2 + 2 * s, self.slot(self.x + s + 1, self.core)).start()
        else:
            self.relay(self.chips - 1, self.slot(self.x + self.steps, self.core)).start()

    def finish(self):
        for k, offset in self.relays():
            self.relay(k, self.slot(self.x + offset, 1 - self.core)).wait_recv()

    def drain(self):
        for d in (0, 1):
            for s in range(self.steps):
                for c in self.parts(d, s):
                    self.ring(d, s, c).wait_send()
        for k, offset in self.relays():
            self.relay(k, self.slot(self.x + offset, self.core)).wait_send()


def kernel(
    n,
    tp,
    tok_ref,
    w_ref,
    gate_ref,
    gain_ref,
    qk_gain_ref,
    sink_ref,
    out_ref,
    tokb,
    nb,
    wb,
    gb,
    kv,
    prev,
    keys_ext,
    values_ext,
    wqb,
    fqb,
    fob,
    wob,
    sgb,
    mixb,
    accb,
    maxb,
    sumb,
    w_send,
    w_recv,
    g_send,
    g_recv,
    kv_send,
    kv_recv,
    prev_send,
    prev_recv,
    *tp_sems,
):
    me = lax.axis_index("sp")
    t = lax.axis_index("tp")
    right, left = lax.rem(me + 1, n), lax.rem(me + n - 1, n)
    chips = tp // 2
    rows, cols = tok_ref.shape
    depth = w_ref.shape[0]
    width = gain_ref.shape[1]
    w_parts = w_recv.shape[2]
    w_rows = depth // w_parts
    last = n // 2 - 1
    tiles = rows // 128
    first_branch = w_ref.shape[1] - cols
    first_merge = first_branch - 2 * cols

    tokens = TpGather(tok_ref, tokb, t, chips, tp_sems[0:4])
    window_outs = TpGather(None, wob, t, chips, tp_sems[4:8])
    forget_outs = TpGather(None, fob, t, chips, tp_sems[8:12])

    barrier = pltpu.get_barrier_semaphore()
    greeted = [
        {"sp": right},
        {"sp": left},
        {"tp": tokens.slot(tokens.x + 1, tokens.core)},
        {"tp": tokens.slot(tokens.x - 1, tokens.core)},
        {"tp": t + 1 - 2 * tokens.core},
    ]
    for device in greeted:
        pl.semaphore_signal(barrier, inc=1, device_id=device, device_id_type=MESH)
    pl.semaphore_wait(barrier, len(greeted))

    def ring_block(d, s):
        return lax.rem(me + n - s, n) if d == 0 else lax.rem(me + s, n)

    def to_next(d):
        return {"sp": right if d == 0 else left}

    def ring_copy(src, dst, send, recv, d):
        return pltpu.make_async_remote_copy(
            src_ref=src,
            dst_ref=dst,
            send_sem=send,
            recv_sem=recv,
            device_id=to_next(d),
            device_id_type=MESH,
        )

    def w_copy(d, s, q, own=False):
        part = pl.ds(q * w_rows, w_rows)
        dst = wb.at[ring_block(d, s), part]
        return ring_copy(w_ref.at[part] if own else dst, dst, w_send.at[d, s, q], w_recv.at[d, s, q], d)

    def g_copy(d, s, own=False):
        dst = gb.at[ring_block(d, s)]
        return ring_copy(gate_ref if own else dst, dst, g_send.at[d, s], g_recv.at[d, s], d)

    kv_parts = kv_recv.shape[2]
    kv_rows = rows // kv_parts

    def kv_copy(d, s, q):
        dst = kv.at[ring_block(d, s), pl.ds(q * kv_rows, kv_rows)]
        return ring_copy(dst, dst, kv_send.at[d, s, q], kv_recv.at[d, s, q], d)

    for d in (0, 1):
        if d == 0 or last > 0:
            g_copy(d, 0, own=True).start()
            for q in range(w_parts):
                w_copy(d, 0, q, own=True).start()
    wb[me] = w_ref[...]
    gb[me] = gate_ref[...]
    tokb[t] = tok_ref[...]

    def normalize():
        tokens.finish()
        for r in range(tiles):
            part = pl.ds(r * 128, 128)
            total = jnp.zeros((128, 1), jnp.float32)
            for k in range(tp):
                x = tokb[k, part].astype(jnp.float32)
                total += jnp.sum(x * x, axis=1, keepdims=True)
            scale = lax.rsqrt(total * (1.0 / width) + epsilon)
            for k in range(tp):
                x = tokb[k, part].astype(jnp.float32)
                nb[part, k * cols : (k + 1) * cols] = (
                    x * scale * gain_ref[:, k * cols : (k + 1) * cols]
                ).astype(jnp.bfloat16)

    def run_at(step, tasks, spacing):
        for k, task in enumerate(tasks):
            at = 1 + k * spacing
            if at <= last:
                pl.when(step == at)(task)

    def run_late(tasks, spacing):
        for k, task in enumerate(tasks):
            if 1 + k * spacing > last:
                task()

    token_tasks = [functools.partial(tokens.advance, s) for s in range(tokens.steps)] + [normalize]
    tokens.begin()

    def w_step(s, carry):
        for q in range(w_parts):
            for d in (0, 1):
                w_copy(d, s - 1, q).wait_recv()
                if d == 0:
                    w_copy(d, s, q).start()
                else:
                    pl.when(s < last)(w_copy(d, s, q).start)
        for d in (0, 1):
            g_copy(d, s - 1).wait_recv()
            if d == 0:
                g_copy(d, s).start()
            else:
                pl.when(s < last)(g_copy(d, s).start)
        run_at(s, token_tasks, 2)
        return carry

    lax.fori_loop(1, last + 1, w_step, 0)
    run_late(token_tasks, 2)
    g_copy(0, last).wait_recv()
    for q in range(w_parts):
        w_copy(0, last, q).wait_recv()

    def project(start, size):
        weights = wb[:, :, start : start + size].reshape(width, size)
        return jnp.dot(nb[...], weights, preferred_element_type=jnp.float32)

    both = project(0, 2 * PAIR)
    kv[me, :, 0:PAIR] = pair_norm(both[:, 0:PAIR], qk_gain_ref[3:4, :]).astype(jnp.bfloat16)
    kv[me, :, PAIR : 2 * PAIR] = both[:, PAIR : 2 * PAIR].astype(jnp.bfloat16)

    def split_heads(dst, query):
        low = low_half(query.shape)
        dst[0] = jnp.where(low, query, 0.0).astype(jnp.bfloat16)
        dst[1] = jnp.where(low, 0.0, query).astype(jnp.bfloat16)

    both = project(2 * PAIR, 2 * PAIR)
    for d in (0, 1):
        for q in range(kv_parts):
            if last > 0 or q == d:
                kv_copy(d, 0, q).start()
    split_heads(fqb, pair_norm(both[:, 0:PAIR], qk_gain_ref[2:3, :]))
    split_heads(wqb, pair_norm(both[:, PAIR : 2 * PAIR], qk_gain_ref[0:1, :]))

    to_log2 = log2e * HEAD ** (-0.5)

    def absorb(block, own):
        for h in (0, 1):
            key_gate = (gb[me, h : h + 1, 0:1] - gb[block, h : h + 1, :]) * log2e
            for r in range(tiles):
                part = pl.ds(r * 128, 128)
                span = (r + 1) * 128 if own else rows
                scores = dot_nt(fqb[h, part], kv[block, 0:span, 0:PAIR]) * to_log2 + key_gate[:, 0:span]
                if own:
                    query_pos = r * 128 + lax.broadcasted_iota(jnp.int32, scores.shape, 0)
                    key_pos = lax.broadcasted_iota(jnp.int32, scores.shape, 1)
                    scores = jnp.where(query_pos >= key_pos, scores, big_negative)
                top = jnp.max(scores, axis=1, keepdims=True)
                if not own:
                    before = maxb[h, part]
                    top = jnp.maximum(before, top)
                weights = jnp.exp2(scores - top)
                partial = weights[:, 0:128]
                for k in range(1, span // 128):
                    partial += weights[:, k * 128 : (k + 1) * 128]
                product = jnp.dot(
                    weights.astype(jnp.bfloat16),
                    kv[block, 0:span, PAIR : 2 * PAIR],
                    preferred_element_type=jnp.float32,
                )
                if not own:
                    shrink = jnp.exp2(before - top)
                    partial += sumb[h, part] * shrink
                    product += accb[h, part] * shrink
                maxb[h, part] = top
                sumb[h, part] = partial
                accb[h, part] = product

    def window_project():
        raw = project(4 * PAIR, PAIR)
        low = low_half(raw.shape)
        mean = jnp.sum(jnp.where(low, raw * raw, 0.0), axis=1, keepdims=True) * (1.0 / HEAD)
        key = raw * lax.rsqrt(mean + epsilon) * qk_gain_ref[1:2, :]
        ext = jnp.where(low, key, raw)
        turned = pltpu.roll(ext, HEAD, 1)
        keys_ext[WINDOW:, :] = jnp.where(low, ext, turned).astype(jnp.bfloat16)
        values_ext[WINDOW:, :] = jnp.where(low, turned, ext).astype(jnp.bfloat16)
        prev[0] = ext[rows - WINDOW :, :].astype(jnp.bfloat16)

    def prev_copy():
        return ring_copy(prev.at[0], prev.at[1], prev_send, prev_recv, 0)

    def window_send():
        prev_copy().start()

    def window_attend():
        prev_copy().wait_recv()
        ext = prev[1].astype(jnp.float32)
        low = low_half(ext.shape)
        turned = pltpu.roll(ext, HEAD, 1)
        keys_ext[0:WINDOW, :] = jnp.where(low, ext, turned).astype(jnp.bfloat16)
        values_ext[0:WINDOW, :] = jnp.where(low, turned, ext).astype(jnp.bfloat16)
        for r in range(tiles):
            part = pl.ds(r * 128, 128)
            outs = []
            for h in (0, 1):
                span = pl.ds(r * 128, 128 + WINDOW)
                scores = dot_nt(wqb[h, part], keys_ext[span, :]) * HEAD ** (-0.5)
                distance = (
                    WINDOW
                    + lax.broadcasted_iota(jnp.int32, scores.shape, 0)
                    - lax.broadcasted_iota(jnp.int32, scores.shape, 1)
                )
                key_pos = (
                    me * rows + r * 128 - WINDOW + lax.broadcasted_iota(jnp.int32, scores.shape, 1)
                )
                valid = (distance >= 0) & (distance < WINDOW) & (key_pos >= 0)
                sink = sink_ref[h]
                top = jnp.maximum(
                    jnp.max(jnp.where(valid, scores, big_negative), axis=1, keepdims=True), sink
                )
                weights = jnp.where(valid, jnp.exp(scores - top), 0.0)
                total = jnp.sum(weights, axis=1, keepdims=True) + jnp.exp(sink - top)
                probs = (weights / total).astype(jnp.bfloat16)
                outs.append(
                    jnp.dot(probs, values_ext[span, :], preferred_element_type=jnp.float32)
                )
            merged = jnp.where(low_half(outs[0].shape), outs[0], outs[1])
            wob[t, part] = merged.astype(jnp.bfloat16)

    def merge_project(b):
        logits = project(first_merge + b * cols, cols)
        sgb[b] = jax.nn.sigmoid(logits)

    def branch_project(buf, b):
        per = n // tp
        high = depth // 2
        total = jnp.zeros((rows, cols), jnp.float32)
        for k in range(tp):
            weights = wb[k * per : (k + 1) * per, b * high : (b + 1) * high, first_branch:].reshape(
                per * high, cols
            )
            total += jnp.dot(buf[k], weights, preferred_element_type=jnp.float32)
        return total

    def window_mix():
        window_outs.finish()
        mixb[...] = sgb[0] * branch_project(wob, 0)

    absorb(me, True)
    tasks = (
        [window_project, window_send, window_attend, window_outs.begin]
        + [functools.partial(window_outs.advance, s) for s in range(window_outs.steps)]
        + [functools.partial(merge_project, b) for b in (0, 1)]
        + [window_mix]
    )

    def kv_step(s, carry):
        for q in range(kv_parts):
            for d in (0, 1):
                kv_copy(d, s - 1, q).wait_recv()
                if q == d:
                    kv_copy(d, s, q).start()
                else:
                    pl.when(s < last)(kv_copy(d, s, q).start)
        run_at(s, tasks, 1)
        pl.when(me >= s)(functools.partial(absorb, lax.rem(me + n - s, n), False))
        pl.when(me + s >= n)(functools.partial(absorb, lax.rem(me + s, n), False))
        return carry

    lax.fori_loop(1, last + 1, kv_step, 0)
    run_late(tasks, 1)
    kv_copy(0, last, 0).wait_recv()
    kv_copy(1, last, 1).wait_recv()
    pl.when(me >= n // 2)(functools.partial(absorb, lax.rem(me + n // 2, n), False))

    for r in range(tiles):
        part = pl.ds(r * 128, 128)
        outs = [accb[h, part] / jnp.sum(sumb[h, part], axis=1, keepdims=True) for h in (0, 1)]
        merged = jnp.where(low_half(outs[0].shape), outs[0], outs[1])
        fob[t, part] = merged.astype(jnp.bfloat16)
    forget_outs.begin()
    for s in range(forget_outs.steps):
        forget_outs.advance(s)
    forget_outs.finish()
    out_ref[...] = (mixb[...] + sgb[1] * branch_project(fob, 1)).astype(jnp.bfloat16)

    def drain_step(s, carry):
        for d in (0, 1):

            def full(d=d):
                g_copy(d, s).wait_send()
                for q in range(w_parts):
                    w_copy(d, s, q).wait_send()

            if d == 0:
                full()
            else:
                pl.when(s < last)(full)
            for q in range(kv_parts):
                if q == d:
                    kv_copy(d, s, q).wait_send()
                else:
                    pl.when(s < last)(kv_copy(d, s, q).wait_send)
        return carry

    lax.fori_loop(0, last + 1, drain_step, 0)
    prev_copy().wait_send()
    for gather in (tokens, window_outs, forget_outs):
        gather.drain()


def on_device(
    n,
    tp,
    tokens,
    norm_gain,
    qk_gain,
    w_query_window,
    w_key_window,
    w_value_window,
    sink_logits,
    w_query_forget,
    w_key_forget,
    w_value_forget,
    gate_cum,
    w_merge,
    w_branch,
):
    rows, cols = tokens.shape
    depth = w_merge.shape[0]
    width = norm_gain.shape[0]
    weights = jnp.concatenate(
        [
            w_key_forget,
            w_value_forget,
            w_query_forget,
            w_query_window,
            w_key_window,
            w_value_window,
            w_merge.reshape(depth, -1),
            w_branch.reshape(depth, -1),
        ],
        axis=1,
    )
    steps, chips = n // 2, tp // 2
    tp_sems = [
        pltpu.SemaphoreType.DMA((2, max(chips // 2, 1), 2)),
        pltpu.SemaphoreType.DMA((2, max(chips // 2, 1), 2)),
        pltpu.SemaphoreType.DMA((chips,)),
        pltpu.SemaphoreType.DMA((chips,)),
    ]
    w_parts, kv_parts = 2, 2
    bf16, f32 = jnp.bfloat16, jnp.float32
    vmem = pl.BlockSpec(memory_space=pltpu.VMEM)
    return pl.pallas_call(
        functools.partial(kernel, n, tp),
        out_shape=jax.ShapeDtypeStruct((rows, cols), bf16),
        in_specs=[vmem] * 5 + [pl.BlockSpec(memory_space=pltpu.SMEM)],
        out_specs=vmem,
        scratch_shapes=[
            pltpu.VMEM((tp, rows, cols), bf16),
            pltpu.VMEM((rows, width), bf16),
            pltpu.VMEM((n, depth, weights.shape[1]), bf16),
            pltpu.VMEM((n, 2, rows), f32),
            pltpu.VMEM((n, rows, 2 * PAIR), bf16),
            pltpu.VMEM((2, WINDOW, PAIR), bf16),
            pltpu.VMEM((WINDOW + rows, PAIR), bf16),
            pltpu.VMEM((WINDOW + rows, PAIR), bf16),
            pltpu.VMEM((2, rows, PAIR), bf16),
            pltpu.VMEM((2, rows, PAIR), bf16),
            pltpu.VMEM((tp, rows, PAIR), bf16),
            pltpu.VMEM((tp, rows, PAIR), bf16),
            pltpu.VMEM((2, rows, cols), f32),
            pltpu.VMEM((rows, cols), f32),
            pltpu.VMEM((2, rows, PAIR), f32),
            pltpu.VMEM((2, rows, 1), f32),
            pltpu.VMEM((2, rows, PAIR), f32),
            pltpu.SemaphoreType.DMA((2, steps, w_parts)),
            pltpu.SemaphoreType.DMA((2, steps, w_parts)),
            pltpu.SemaphoreType.DMA((2, steps)),
            pltpu.SemaphoreType.DMA((2, steps)),
            pltpu.SemaphoreType.DMA((2, steps, kv_parts)),
            pltpu.SemaphoreType.DMA((2, steps, kv_parts)),
            pltpu.SemaphoreType.DMA,
            pltpu.SemaphoreType.DMA,
        ]
        + tp_sems * 3,
        compiler_params=pltpu.CompilerParams(
            collective_id=0, has_side_effects=True, vmem_limit_bytes=60 * 1024 * 1024
        ),
    )(
        tokens,
        weights,
        gate_cum.T,
        norm_gain.reshape(1, width),
        jnp.concatenate([qk_gain, qk_gain], axis=1),
        sink_logits,
    )


def solution(mesh):
    return jax.shard_map(
        functools.partial(on_device, mesh.shape["sp"], mesh.shape["tp"]),
        mesh=mesh,
        in_specs=(
            P(("grp", "sp"), "tp"),
            P(),
            P(),
            P("sp", "tp"),
            P("sp", "tp"),
            P("sp", "tp"),
            P("tp"),
            P("sp", "tp"),
            P("sp", "tp"),
            P("sp", "tp"),
            P(("grp", "sp"), "tp"),
            P("sp", None, "tp"),
            P(None, "sp", "tp"),
        ),
        out_specs=P(("grp", "sp"), "tp"),
        check_vma=False,
    )
```

time: 460 us -> 220 us (0.48)
  the two profiles are of different devices: /device:TPU:34 before, /device:TPU:33 now
where the time goes in v1:
time: 220 us
  Pallas kernels  215 us (98%)
  local copies, waits for them, and re-layouts  4.01 us (2%)
    pallas_call x1, Pallas kernels, on_device(): pl.pallas_call(functools.partial(kernel, n, tp), out_shape=jax.ShapeDtype...  215 us

profile of v1, /device:TPU:33, one launch (start us, length us, event | category | flops | bytes accessed | tf_op | source)
XLA Modules:
  0.0 219.6 jit_solution(6620094784386378301)
XLA Ops:
  0.0 0.0 copy-start.7
  0.0 0.7 copy-done.7
  0.7 0.7 pad_maximum_fusion.qk_gain_ref
  1.3 0.0 copy-start
  1.3 0.0 copy-start.1
  1.3 0.0 copy-start.2
  1.4 0.0 copy-start.3
  1.4 0.0 copy-start.4
  1.4 0.0 copy-start.5
  1.4 0.0 copy-start.6
  1.4 0.9 copy.14
  2.3 0.0 copy-done
  2.3 0.0 copy-done.1
  2.3 0.0 copy-done.2
  2.3 0.0 copy-done.3
  2.3 0.0 copy-done.4
  2.4 0.0 copy-done.5
  2.4 0.0 copy-done.6
  2.4 0.8 concatenate.6.w_ref
  3.1 214.8 %shard_map.127 = bf16[384,256]{1,0:T(8,128)(2,1)} custom-call(bf16[384,256]{1,0:T(8,128)(2,1)} %tok_ref.1, bf16[64,1408]{1,0:T(8,128)(2,1)} %concatenate.6.w_ref, f32[2,384]{1,0:T(2,128)} %bitcast.9, f32[1,2048]{1,0:T(1,128)} %bitcast.8, f32[4,128]{1,0:T(4,128)} %pad_maximum_fusion.qk_gain_ref, f32[2]{0:T(128)} %sink_ref.1), custom_call_target="tpu_custom_call" | custom-call | tf_op jit(solution)/shard_map/pallas_call | solution.py:511
  217.9 1.6 copy.16
Async XLA Ops:
  0.0 0.7 copy-start.7
  1.3 1.0 copy-start
  1.3 1.0 copy-start.1
  1.3 1.0 copy-start.2
  1.4 1.0 copy-start.3
  1.4 1.0 copy-start.4
  1.4 1.0 copy-start.5
  1.4 1.0 copy-start.6

commit v2 on v1

--- a/solution.py
+++ b/solution.py
@@ -50,7 +50,7 @@
         return self.slot(self.x - s if d == 0 else self.x + s, self.core)
 
     def parts(self, d, s):
-        return (0, 1) if s < self.steps - 1 else (d,)
+        return (d, 1 - d) if s < self.steps - 1 else (d,)
 
     def ring(self, d, s, c):
         block = self.block(d, s)
@@ -92,8 +92,9 @@
         self.relay(0, self.slot(self.x, self.core)).start()
 
     def advance(self, s):
-        for d in (0, 1):
-            for c in self.parts(d, s):
+        for k in range(len(self.parts(0, s))):
+            for d in (0, 1):
+                c = self.parts(d, s)[k]
                 self.ring(d, s, c).wait_recv()
                 if s + 1 < self.steps and c in self.parts(d, s + 1):
                     self.ring(d, s + 1, c).start()
@@ -119,6 +120,7 @@
 def kernel(
     n,
     tp,
+    share,
     tok_ref,
     w_ref,
     gate_ref,
@@ -130,7 +132,9 @@
     nb,
     wb,
     gb,
-    kv,
+    gates,
+    kb,
+    vb,
     prev,
     keys_ext,
     values_ext,
@@ -145,6 +149,8 @@
     sumb,
     w_send,
     w_recv,
+    pair_send,
+    pair_recv,
     g_send,
     g_recv,
     kv_send,
@@ -160,8 +166,11 @@
     rows, cols = tok_ref.shape
     depth = w_ref.shape[0]
     width = gain_ref.shape[1]
-    w_parts = w_recv.shape[2]
-    w_rows = depth // w_parts
+    quarter = depth // 4
+    group = lax.axis_index("grp")
+    odd = group % 2
+    quarters = [2 + odd, 0, 1] if share else [0, 1, 2, 3]
+    cuts = [0, w_ref.shape[1] - 3 * tok_ref.shape[1], w_ref.shape[1]]
     last = n // 2 - 1
     tiles = rows // 128
     first_branch = w_ref.shape[1] - cols
@@ -179,6 +188,8 @@
         {"tp": tokens.slot(tokens.x - 1, tokens.core)},
         {"tp": t + 1 - 2 * tokens.core},
     ]
+    if share:
+        greeted.append({"grp": group + 1 - 2 * odd})
     for device in greeted:
         pl.semaphore_signal(barrier, inc=1, device_id=device, device_id_type=MESH)
     pl.semaphore_wait(barrier, len(greeted))
@@ -199,27 +210,52 @@
             device_id_type=MESH,
         )
 
-    def w_copy(d, s, q, own=False):
-        part = pl.ds(q * w_rows, w_rows)
-        dst = wb.at[ring_block(d, s), part]
-        return ring_copy(w_ref.at[part] if own else dst, dst, w_send.at[d, s, q], w_recv.at[d, s, q], d)
+    def quarter_rows(k):
+        return pl.ds(k * quarter if isinstance(k, int) else pl.multiple_of(k * quarter, 16), quarter)
+
+    def w_copy(d, s, q, c, own=False):
+        rows_of, cols_of = quarter_rows(quarters[q]), pl.ds(cuts[c], cuts[c + 1] - cuts[c])
+        dst = wb.at[ring_block(d, s), rows_of, cols_of]
+        src = w_ref.at[rows_of, cols_of] if own else dst
+        k = 2 * q + c
+        return ring_copy(src, dst, w_send.at[d, s, k], w_recv.at[d, s, k], d)
+
+    def pair_copy(d, s):
+        block = wb.at[ring_block(d, s + 1), quarter_rows(quarters[0])]
+        return pltpu.make_async_remote_copy(
+            src_ref=block,
+            dst_ref=block,
+            send_sem=pair_send.at[d, s],
+            recv_sem=pair_recv.at[d, s],
+            device_id={"grp": group + 1 - 2 * odd},
+            device_id_type=MESH,
+        )
 
     def g_copy(d, s, own=False):
         dst = gb.at[ring_block(d, s)]
         return ring_copy(gate_ref if own else dst, dst, g_send.at[d, s], g_recv.at[d, s], d)
 
-    kv_parts = kv_recv.shape[2]
-    kv_rows = rows // kv_parts
+    kv_parts = 4
 
     def kv_copy(d, s, q):
-        dst = kv.at[ring_block(d, s), pl.ds(q * kv_rows, kv_rows)]
+        block = ring_block(d, s)
+        if q % 2 == 0:
+            dst = kb.at[block, pl.ds(q // 2 * (rows // 2), rows // 2)]
+        else:
+            dst = vb.at[block, pl.ds(q // 2 * HEAD, HEAD)]
         return ring_copy(dst, dst, kv_send.at[d, s, q], kv_recv.at[d, s, q], d)
+
+    def halfway(d, q):
+        return q // 2 == d
 
     for d in (0, 1):
         if d == 0 or last > 0:
             g_copy(d, 0, own=True).start()
-            for q in range(w_parts):
-                w_copy(d, 0, q, own=True).start()
+    for q in range(len(quarters)):
+        for c in (0, 1):
+            for d in (0, 1):
+                if d == 0 or last > 0:
+                    w_copy(d, 0, q, c, own=True).start()
     wb[me] = w_ref[...]
     gb[me] = gate_ref[...]
     tokb[t] = tok_ref[...]
@@ -253,36 +289,59 @@
     token_tasks = [functools.partial(tokens.advance, s) for s in range(tokens.steps)] + [normalize]
     tokens.begin()
 
+    def turn_gates(block):
+        pair = gb[block]
+        gates[block, :, 0:8] = jnp.transpose(jnp.concatenate([pair] * 4, axis=0)) * log2e
+
     def w_step(s, carry):
-        for q in range(w_parts):
-            for d in (0, 1):
-                w_copy(d, s - 1, q).wait_recv()
-                if d == 0:
-                    w_copy(d, s, q).start()
-                else:
-                    pl.when(s < last)(w_copy(d, s, q).start)
+        for q in range(len(quarters)):
+            for c in (0, 1):
+                for d in (0, 1):
+                    w_copy(d, s - 1, q, c).wait_recv()
+                    if d == 0:
+                        w_copy(d, s, q, c).start()
+                    else:
+                        pl.when(s < last)(w_copy(d, s, q, c).start)
+            if share and q == 0:
+                for d in (0, 1):
+                    pair_copy(d, s - 1).start()
         for d in (0, 1):
             g_copy(d, s - 1).wait_recv()
             if d == 0:
                 g_copy(d, s).start()
             else:
                 pl.when(s < last)(g_copy(d, s).start)
+        turn_gates(ring_block(0, s))
+        turn_gates(ring_block(1, s))
         run_at(s, token_tasks, 2)
         return carry
 
     lax.fori_loop(1, last + 1, w_step, 0)
     run_late(token_tasks, 2)
+    for q in range(len(quarters)):
+        for c in (0, 1):
+            w_copy(0, last, q, c).wait_recv()
+        if share and q == 0:
+            pair_copy(0, last).start()
     g_copy(0, last).wait_recv()
-    for q in range(w_parts):
-        w_copy(0, last, q).wait_recv()
+    turn_gates(ring_block(0, last + 1))
+    turn_gates(me)
+    if share:
+
+        def pair_step(s, carry):
+            pair_copy(0, s).wait_recv()
+            pl.when(s < last)(pair_copy(1, s).wait_recv)
+            return carry
+
+        lax.fori_loop(0, last + 1, pair_step, 0)
 
     def project(start, size):
         weights = wb[:, :, start : start + size].reshape(width, size)
         return jnp.dot(nb[...], weights, preferred_element_type=jnp.float32)
 
     both = project(0, 2 * PAIR)
-    kv[me, :, 0:PAIR] = pair_norm(both[:, 0:PAIR], qk_gain_ref[3:4, :]).astype(jnp.bfloat16)
-    kv[me, :, PAIR : 2 * PAIR] = both[:, PAIR : 2 * PAIR].astype(jnp.bfloat16)
+    kb[me] = pair_norm(both[:, 0:PAIR], qk_gain_ref[3:4, :]).astype(jnp.bfloat16)
+    vb[me] = jnp.transpose(both[:, PAIR : 2 * PAIR]).astype(jnp.bfloat16)
 
     def split_heads(dst, query):
         low = low_half(query.shape)
@@ -290,46 +349,49 @@
         dst[1] = jnp.where(low, 0.0, query).astype(jnp.bfloat16)
 
     both = project(2 * PAIR, 2 * PAIR)
-    for d in (0, 1):
-        for q in range(kv_parts):
-            if last > 0 or q == d:
+    for q in range(kv_parts):
+        for d in (0, 1):
+            if last > 0 or halfway(d, q):
                 kv_copy(d, 0, q).start()
-    split_heads(fqb, pair_norm(both[:, 0:PAIR], qk_gain_ref[2:3, :]))
+    turned = jnp.transpose(pair_norm(both[:, 0:PAIR], qk_gain_ref[2:3, :]))
+    first = lax.broadcasted_iota(jnp.int32, turned.shape, 0) < HEAD
+    fqb[0] = jnp.where(first, turned, 0.0).astype(jnp.bfloat16)
+    fqb[1] = jnp.where(first, 0.0, turned).astype(jnp.bfloat16)
     split_heads(wqb, pair_norm(both[:, PAIR : 2 * PAIR], qk_gain_ref[0:1, :]))
 
     to_log2 = log2e * HEAD ** (-0.5)
 
     def absorb(block, own):
+        scores = []
         for h in (0, 1):
-            key_gate = (gb[me, h : h + 1, 0:1] - gb[block, h : h + 1, :]) * log2e
-            for r in range(tiles):
-                part = pl.ds(r * 128, 128)
-                span = (r + 1) * 128 if own else rows
-                scores = dot_nt(fqb[h, part], kv[block, 0:span, 0:PAIR]) * to_log2 + key_gate[:, 0:span]
-                if own:
-                    query_pos = r * 128 + lax.broadcasted_iota(jnp.int32, scores.shape, 0)
-                    key_pos = lax.broadcasted_iota(jnp.int32, scores.shape, 1)
-                    scores = jnp.where(query_pos >= key_pos, scores, big_negative)
-                top = jnp.max(scores, axis=1, keepdims=True)
-                if not own:
-                    before = maxb[h, part]
-                    top = jnp.maximum(before, top)
-                weights = jnp.exp2(scores - top)
-                partial = weights[:, 0:128]
-                for k in range(1, span // 128):
-                    partial += weights[:, k * 128 : (k + 1) * 128]
-                product = jnp.dot(
-                    weights.astype(jnp.bfloat16),
-                    kv[block, 0:span, PAIR : 2 * PAIR],
-                    preferred_element_type=jnp.float32,
-                )
-                if not own:
-                    shrink = jnp.exp2(before - top)
-                    partial += sumb[h, part] * shrink
-                    product += accb[h, part] * shrink
-                maxb[h, part] = top
-                sumb[h, part] = partial
-                accb[h, part] = product
+            key_gate = gates[me, 0:1, h : h + 1] - gates[block, :, h : h + 1]
+            both = jnp.dot(kb[block], fqb[h], preferred_element_type=jnp.float32) * to_log2 + key_gate
+            if own:
+                key_pos = lax.broadcasted_iota(jnp.int32, both.shape, 0)
+                query_pos = lax.broadcasted_iota(jnp.int32, both.shape, 1)
+                both = jnp.where(query_pos >= key_pos, both, big_negative)
+            scores.append(both)
+        parts = []
+        for h in (0, 1):
+            top = jnp.max(scores[h], axis=0, keepdims=True)
+            if not own:
+                before = maxb[h]
+                top = jnp.maximum(before, top)
+            weights = jnp.exp2(scores[h] - top)
+            total = jnp.sum(weights, axis=0, keepdims=True)
+            shrink = None
+            if not own:
+                shrink = jnp.exp2(before - top)
+                total += sumb[h] * shrink
+            maxb[h] = top
+            sumb[h] = total
+            parts.append((weights.astype(jnp.bfloat16), shrink))
+        for h, (weights, shrink) in enumerate(parts):
+            head = pl.ds(h * HEAD, HEAD)
+            product = jnp.dot(vb[block, head], weights, preferred_element_type=jnp.float32)
+            if not own:
+                product += accb[head] * shrink
+            accb[head] = product
 
     def window_project():
         raw = project(4 * PAIR, PAIR)
@@ -414,7 +476,7 @@
         for q in range(kv_parts):
             for d in (0, 1):
                 kv_copy(d, s - 1, q).wait_recv()
-                if q == d:
+                if halfway(d, q):
                     kv_copy(d, s, q).start()
                 else:
                     pl.when(s < last)(kv_copy(d, s, q).start)
@@ -425,15 +487,16 @@
 
     lax.fori_loop(1, last + 1, kv_step, 0)
     run_late(tasks, 1)
-    kv_copy(0, last, 0).wait_recv()
-    kv_copy(1, last, 1).wait_recv()
+    for d in (0, 1):
+        for q in range(kv_parts):
+            if halfway(d, q):
+                kv_copy(d, last, q).wait_recv()
     pl.when(me >= n // 2)(functools.partial(absorb, lax.rem(me + n // 2, n), False))
 
-    for r in range(tiles):
-        part = pl.ds(r * 128, 128)
-        outs = [accb[h, part] / jnp.sum(sumb[h, part], axis=1, keepdims=True) for h in (0, 1)]
-        merged = jnp.where(low_half(outs[0].shape), outs[0], outs[1])
-        fob[t, part] = merged.astype(jnp.bfloat16)
+    for h in (0, 1):
+        head = pl.ds(h * HEAD, HEAD)
+        accb[head] = accb[head] / sumb[h]
+    fob[t] = jnp.transpose(accb[...]).astype(jnp.bfloat16)
     forget_outs.begin()
     for s in range(forget_outs.steps):
         forget_outs.advance(s)
@@ -445,15 +508,18 @@
 
             def full(d=d):
                 g_copy(d, s).wait_send()
-                for q in range(w_parts):
-                    w_copy(d, s, q).wait_send()
+                for q in range(len(quarters)):
+                    for c in (0, 1):
+                        w_copy(d, s, q, c).wait_send()
+                if share:
+                    pair_copy(d, s).wait_send()
 
             if d == 0:
                 full()
             else:
                 pl.when(s < last)(full)
             for q in range(kv_parts):
-                if q == d:
+                if halfway(d, q):
                     kv_copy(d, s, q).wait_send()
                 else:
                     pl.when(s < last)(kv_copy(d, s, q).wait_send)
@@ -468,6 +534,7 @@
 def on_device(
     n,
     tp,
+    share,
     tokens,
     norm_gain,
     qk_gain,
@@ -505,11 +572,11 @@
         pltpu.SemaphoreType.DMA((chips,)),
         pltpu.SemaphoreType.DMA((chips,)),
     ]
-    w_parts, kv_parts = 2, 2
+    w_pieces, kv_pieces = (6 if share else 8), 4
     bf16, f32 = jnp.bfloat16, jnp.float32
     vmem = pl.BlockSpec(memory_space=pltpu.VMEM)
     return pl.pallas_call(
-        functools.partial(kernel, n, tp),
+        functools.partial(kernel, n, tp, share),
         out_shape=jax.ShapeDtypeStruct((rows, cols), bf16),
         in_specs=[vmem] * 5 + [pl.BlockSpec(memory_space=pltpu.SMEM)],
         out_specs=vmem,
@@ -518,25 +585,29 @@
             pltpu.VMEM((rows, width), bf16),
             pltpu.VMEM((n, depth, weights.shape[1]), bf16),
             pltpu.VMEM((n, 2, rows), f32),
-            pltpu.VMEM((n, rows, 2 * PAIR), bf16),
+            pltpu.VMEM((n, rows, 128), f32),
+            pltpu.VMEM((n, rows, PAIR), bf16),
+            pltpu.VMEM((n, PAIR, rows), bf16),
             pltpu.VMEM((2, WINDOW, PAIR), bf16),
             pltpu.VMEM((WINDOW + rows, PAIR), bf16),
             pltpu.VMEM((WINDOW + rows, PAIR), bf16),
             pltpu.VMEM((2, rows, PAIR), bf16),
-            pltpu.VMEM((2, rows, PAIR), bf16),
+            pltpu.VMEM((2, PAIR, rows), bf16),
             pltpu.VMEM((tp, rows, PAIR), bf16),
             pltpu.VMEM((tp, rows, PAIR), bf16),
             pltpu.VMEM((2, rows, cols), f32),
             pltpu.VMEM((rows, cols), f32),
-            pltpu.VMEM((2, rows, PAIR), f32),
-            pltpu.VMEM((2, rows, 1), f32),
-            pltpu.VMEM((2, rows, PAIR), f32),
-            pltpu.SemaphoreType.DMA((2, steps, w_parts)),
-            pltpu.SemaphoreType.DMA((2, steps, w_parts)),
+            pltpu.VMEM((PAIR, rows), f32),
+            pltpu.VMEM((2, 1, rows), f32),
+            pltpu.VMEM((2, 1, rows), f32),
+            pltpu.SemaphoreType.DMA((2, steps, w_pieces)),
+            pltpu.SemaphoreType.DMA((2, steps, w_pieces)),
             pltpu.SemaphoreType.DMA((2, steps)),
             pltpu.SemaphoreType.DMA((2, steps)),
-            pltpu.SemaphoreType.DMA((2, steps, kv_parts)),
-            pltpu.SemaphoreType.DMA((2, steps, kv_parts)),
+            pltpu.SemaphoreType.DMA((2, steps)),
+            pltpu.SemaphoreType.DMA((2, steps)),
+            pltpu.SemaphoreType.DMA((2, steps, kv_pieces)),
+            pltpu.SemaphoreType.DMA((2, steps, kv_pieces)),
             pltpu.SemaphoreType.DMA,
             pltpu.SemaphoreType.DMA,
         ]
@@ -556,7 +627,9 @@
 
 def solution(mesh):
     return jax.shard_map(
-        functools.partial(on_device, mesh.shape["sp"], mesh.shape["tp"]),
+        functools.partial(
+            on_device, mesh.shape["sp"], mesh.shape["tp"], mesh.shape["grp"] % 2 == 0
+        ),
         mesh=mesh,
         in_specs=(
             P(("grp", "sp"), "tp"),

time: 220 us -> 197 us (0.90)
  Pallas kernels: 215 us -> 192 us
    pallas_call x1, Pallas kernels: 215 us -> 192 us  [on_device(): pl.pallas_call(functools.partial(kernel, n, tp, share), out_shape=jax.Sha...]
where the time goes in v2:
time: 197 us
  Pallas kernels  192 us (97%)
  local copies, waits for them, and re-layouts  4.01 us (2%)
    pallas_call x1, Pallas kernels, on_device(): pl.pallas_call(functools.partial(kernel, n, tp, share), out_shape=jax.Sha...  192 us

profile of v2, /device:TPU:33, one launch (start us, length us, event | category | flops | bytes accessed | tf_op | source)
XLA Modules:
  0.0 197.1 jit_solution(11782525978951719280)
XLA Ops:
  0.0 0.0 copy-start.7
  0.0 0.7 copy-done.7
  0.7 0.7 pad_maximum_fusion.qk_gain_ref
  1.3 0.0 copy-start
  1.3 0.0 copy-start.1
  1.3 0.0 copy-start.2
  1.4 0.0 copy-start.3
  1.4 0.0 copy-start.4
  1.4 0.0 copy-start.5
  1.4 0.0 copy-start.6
  1.4 0.9 copy.14
  2.3 0.0 copy-done
  2.3 0.0 copy-done.1
  2.3 0.0 copy-done.2
  2.3 0.0 copy-done.3
  2.3 0.0 copy-done.4
  2.4 0.0 copy-done.5
  2.4 0.0 copy-done.6
  2.4 0.8 concatenate.6.w_ref
  3.1 192.4 %shard_map.127 = bf16[384,256]{1,0:T(8,128)(2,1)} custom-call(bf16[384,256]{1,0:T(8,128)(2,1)} %tok_ref.1, bf16[64,1408]{1,0:T(8,128)(2,1)} %concatenate.6.w_ref, f32[2,384]{1,0:T(2,128)} %bitcast.9, f32[1,2048]{1,0:T(1,128)} %bitcast.8, f32[4,128]{1,0:T(4,128)} %pad_maximum_fusion.qk_gain_ref, f32[2]{0:T(128)} %sink_ref.1), custom_call_target="tpu_custom_call" | custom-call | tf_op jit(solution)/shard_map/pallas_call | solution.py:578
  195.5 1.6 copy.16
Async XLA Ops:
  0.0 0.7 copy-start.7
  1.3 1.0 copy-start
  1.3 1.0 copy-start.1
  1.3 1.0 copy-start.2
  1.4 1.0 copy-start.3
  1.4 1.0 copy-start.4
  1.4 1.0 copy-start.5
  1.4 1.0 copy-start.6

commit v3 on v2

--- a/solution.py
+++ b/solution.py
@@ -132,7 +132,6 @@
     nb,
     wb,
     gb,
-    gates,
     kb,
     vb,
     prev,
@@ -176,6 +175,10 @@
     first_branch = w_ref.shape[1] - cols
     first_merge = first_branch - 2 * cols
 
+    def head_gain(k):
+        gain = qk_gain_ref[k : k + 1, :]
+        return jnp.concatenate([gain, gain], axis=1)
+
     tokens = TpGather(tok_ref, tokb, t, chips, tp_sems[0:4])
     window_outs = TpGather(None, wob, t, chips, tp_sems[4:8])
     forget_outs = TpGather(None, fob, t, chips, tp_sems[8:12])
@@ -248,9 +251,6 @@
     def halfway(d, q):
         return q // 2 == d
 
-    for d in (0, 1):
-        if d == 0 or last > 0:
-            g_copy(d, 0, own=True).start()
     for q in range(len(quarters)):
         for c in (0, 1):
             for d in (0, 1):
@@ -277,21 +277,17 @@
 
     def run_at(step, tasks, spacing):
         for k, task in enumerate(tasks):
-            at = 1 + k * spacing
+            at = spacing * (1 + k)
             if at <= last:
                 pl.when(step == at)(task)
 
     def run_late(tasks, spacing):
         for k, task in enumerate(tasks):
-            if 1 + k * spacing > last:
+            if spacing * (1 + k) > last:
                 task()
 
     token_tasks = [functools.partial(tokens.advance, s) for s in range(tokens.steps)] + [normalize]
     tokens.begin()
-
-    def turn_gates(block):
-        pair = gb[block]
-        gates[block, :, 0:8] = jnp.transpose(jnp.concatenate([pair] * 4, axis=0)) * log2e
 
     def w_step(s, carry):
         for q in range(len(quarters)):
@@ -305,27 +301,16 @@
             if share and q == 0:
                 for d in (0, 1):
                     pair_copy(d, s - 1).start()
-        for d in (0, 1):
-            g_copy(d, s - 1).wait_recv()
-            if d == 0:
-                g_copy(d, s).start()
-            else:
-                pl.when(s < last)(g_copy(d, s).start)
-        turn_gates(ring_block(0, s))
-        turn_gates(ring_block(1, s))
-        run_at(s, token_tasks, 2)
+        run_at(s, token_tasks, 3)
         return carry
 
     lax.fori_loop(1, last + 1, w_step, 0)
-    run_late(token_tasks, 2)
+    run_late(token_tasks, 3)
     for q in range(len(quarters)):
         for c in (0, 1):
             w_copy(0, last, q, c).wait_recv()
         if share and q == 0:
             pair_copy(0, last).start()
-    g_copy(0, last).wait_recv()
-    turn_gates(ring_block(0, last + 1))
-    turn_gates(me)
     if share:
 
         def pair_step(s, carry):
@@ -340,7 +325,10 @@
         return jnp.dot(nb[...], weights, preferred_element_type=jnp.float32)
 
     both = project(0, 2 * PAIR)
-    kb[me] = pair_norm(both[:, 0:PAIR], qk_gain_ref[3:4, :]).astype(jnp.bfloat16)
+    for d in (0, 1):
+        if d == 0 or last > 0:
+            g_copy(d, 0, own=True).start()
+    kb[me] = pair_norm(both[:, 0:PAIR], head_gain(3)).astype(jnp.bfloat16)
     vb[me] = jnp.transpose(both[:, PAIR : 2 * PAIR]).astype(jnp.bfloat16)
 
     def split_heads(dst, query):
@@ -348,23 +336,29 @@
         dst[0] = jnp.where(low, query, 0.0).astype(jnp.bfloat16)
         dst[1] = jnp.where(low, 0.0, query).astype(jnp.bfloat16)
 
+    def kv_begin(pieces):
+        for q in pieces:
+            for d in (0, 1):
+                if last > 0 or halfway(d, q):
+                    kv_copy(d, 0, q).start()
+
+    kv_begin((0, 2))
     both = project(2 * PAIR, 2 * PAIR)
-    for q in range(kv_parts):
-        for d in (0, 1):
-            if last > 0 or halfway(d, q):
-                kv_copy(d, 0, q).start()
-    turned = jnp.transpose(pair_norm(both[:, 0:PAIR], qk_gain_ref[2:3, :]))
+    kv_begin((1, 3))
+    turned = jnp.transpose(pair_norm(both[:, 0:PAIR], head_gain(2)))
     first = lax.broadcasted_iota(jnp.int32, turned.shape, 0) < HEAD
     fqb[0] = jnp.where(first, turned, 0.0).astype(jnp.bfloat16)
     fqb[1] = jnp.where(first, 0.0, turned).astype(jnp.bfloat16)
-    split_heads(wqb, pair_norm(both[:, PAIR : 2 * PAIR], qk_gain_ref[0:1, :]))
+    split_heads(wqb, pair_norm(both[:, PAIR : 2 * PAIR], head_gain(0)))
 
     to_log2 = log2e * HEAD ** (-0.5)
 
     def absorb(block, own):
         scores = []
+        relative = (gb[me][:, 0:1] - gb[block]) * log2e
+        turned = jnp.transpose(jnp.concatenate([relative] * 4, axis=0))
         for h in (0, 1):
-            key_gate = gates[me, 0:1, h : h + 1] - gates[block, :, h : h + 1]
+            key_gate = turned[:, h : h + 1]
             both = jnp.dot(kb[block], fqb[h], preferred_element_type=jnp.float32) * to_log2 + key_gate
             if own:
                 key_pos = lax.broadcasted_iota(jnp.int32, both.shape, 0)
@@ -397,7 +391,7 @@
         raw = project(4 * PAIR, PAIR)
         low = low_half(raw.shape)
         mean = jnp.sum(jnp.where(low, raw * raw, 0.0), axis=1, keepdims=True) * (1.0 / HEAD)
-        key = raw * lax.rsqrt(mean + epsilon) * qk_gain_ref[1:2, :]
+        key = raw * lax.rsqrt(mean + epsilon) * head_gain(1)
         ext = jnp.where(low, key, raw)
         turned = pltpu.roll(ext, HEAD, 1)
         keys_ext[WINDOW:, :] = jnp.where(low, ext, turned).astype(jnp.bfloat16)
@@ -466,13 +460,19 @@
 
     absorb(me, True)
     tasks = (
-        [window_project, window_send, window_attend, window_outs.begin]
+        [window_project, window_send, window_attend, window_outs.begin, lambda: None]
         + [functools.partial(window_outs.advance, s) for s in range(window_outs.steps)]
         + [functools.partial(merge_project, b) for b in (0, 1)]
         + [window_mix]
     )
 
     def kv_step(s, carry):
+        for d in (0, 1):
+            g_copy(d, s - 1).wait_recv()
+            if d == 0:
+                g_copy(d, s).start()
+            else:
+                pl.when(s < last)(g_copy(d, s).start)
         for q in range(kv_parts):
             for d in (0, 1):
                 kv_copy(d, s - 1, q).wait_recv()
@@ -487,6 +487,7 @@
 
     lax.fori_loop(1, last + 1, kv_step, 0)
     run_late(tasks, 1)
+    g_copy(0, last).wait_recv()
     for d in (0, 1):
         for q in range(kv_parts):
             if halfway(d, q):
@@ -585,7 +586,6 @@
             pltpu.VMEM((rows, width), bf16),
             pltpu.VMEM((n, depth, weights.shape[1]), bf16),
             pltpu.VMEM((n, 2, rows), f32),
-            pltpu.VMEM((n, rows, 128), f32),
             pltpu.VMEM((n, rows, PAIR), bf16),
             pltpu.VMEM((n, PAIR, rows), bf16),
             pltpu.VMEM((2, WINDOW, PAIR), bf16),
@@ -620,7 +620,7 @@
         weights,
         gate_cum.T,
         norm_gain.reshape(1, width),
-        jnp.concatenate([qk_gain, qk_gain], axis=1),
+        qk_gain,
         sink_logits,
     )
 

time: 197 us -> 197 us (level)
  no operation moved by 1% of the time
where the time goes in v3:
time: 197 us; the launch traced here: 196 us
  Pallas kernels  193 us (98%)
  local copies, waits for them, and re-layouts  3.32 us (2%)
    pallas_call x1, Pallas kernels, on_device(): pl.pallas_call(functools.partial(kernel, n, tp, share), out_shape=jax.Sha...  193 us

profile of v3, /device:TPU:33, one launch (start us, length us, event | category | flops | bytes accessed | tf_op | source)
XLA Modules:
  0.0 196.4 jit_solution(3896527298810136550)
XLA Ops:
  0.0 0.0 copy-start
  0.0 0.0 copy-start.1
  0.0 0.0 copy-start.2
  0.0 0.0 copy-start.3
  0.0 0.0 copy-start.4
  0.0 0.0 copy-start.5
  0.0 0.0 copy-start.6
  0.0 0.9 copy.14
  1.0 0.0 copy-done
  1.0 0.0 copy-done.1
  1.0 0.0 copy-done.2
  1.0 0.0 copy-done.3
  1.0 0.0 copy-done.4
  1.0 0.0 copy-done.5
  1.0 0.0 copy-done.6
  1.0 0.8 concatenate.3.w_ref
  1.8 192.9 %shard_map.127 = bf16[384,256]{1,0:T(8,128)(2,1)} custom-call(bf16[384,256]{1,0:T(8,128)(2,1)} %tok_ref.1, bf16[64,1408]{1,0:T(8,128)(2,1)} %concatenate.3.w_ref, f32[2,384]{1,0:T(2,128)} %bitcast.9, f32[1,2048]{1,0:T(1,128)} %bitcast.8, f32[4,64]{1,0:T(4,128)} %qk_gain_ref.1, f32[2]{0:T(128)} %sink_ref.1), custom_call_target="tpu_custom_call" | custom-call | tf_op jit(solution)/shard_map/pallas_call | solution.py:579
  194.7 1.6 copy.16
Async XLA Ops:
  0.0 1.0 copy-start
  0.0 1.0 copy-start.1
  0.0 1.0 copy-start.2
  0.0 1.0 copy-start.3
  0.0 1.0 copy-start.4
  0.0 1.0 copy-start.5
  0.0 1.0 copy-start.6
